TPU v7x, 512 devices: a 4x2x32 block of a 4x8x32 slice. The times are simulated.
512 devices in a mesh: grp: 2 (over y), ep: 64 (over z, core), tp: 4 (over x).
Axes of the slice: x: 4, y: 2, z: 32, core: 2. Of those that a mesh axis runs over, the one named last changes fastest.
The devices are a block of a 4x8x32 slice.
Arguments:
- tokens: bfloat16 [24576, 2048], P(('grp', 'ep')), parts along dimension 0, may hold values from -6 to 6
- norm_gain: float32 [2048], replicated, may hold values from 0.1 to 1.9
- w_gate: bfloat16 [64, 2048, 1024], P('ep', None, 'tp'), may hold values from -0.3125 to 0.3125
- w_up: bfloat16 [64, 2048, 1024], P('ep', None, 'tp'), may hold values from -0.3125 to 0.3125
- w_down: bfloat16 [64, 1024, 2048], P('ep', 'tp'), may hold values from -0.09375 to 0.09375
- expert_ids: int32 [24576, 4], P(('grp', 'ep')), parts along dimension 0, may hold values from 0 to 63, all different within a row; in each aligned block of 192 rows (0 to 191, 192 to 383, ...) at most 16 rows name the same one
- gate_weights: float32 [24576, 4], P(('grp', 'ep')), parts along dimension 0, may hold values from 0.1 to 1
Outputs:
- mixed: bfloat16 [24576, 2048], P(('grp', 'ep'), 'tp'), parts along dimension 0
There are 2 independent parts, one for each index of `grp`. A program takes and returns all parts, laid end to end along the dimension named above; an argument that names none is the same for every part. Nothing has to cross between parts.
Inputs may be any that keep to these rules, and one draw needn't show every extreme that they name: `expert_ids`: each row names 4 different experts; among the rows of one index of ep, no expert is named by more than 16 rows, a bound that some block reaches.
All inputs are finite; a program needn't handle non-finite values.
Results may differ from a plain program's by a relative error of at most 0.012.
Values may be sent and summed in bfloat16 or wider, within the bound.
A program may use at most 64 MiB of HBM per device.

v0:
```python
import jax
import jax.numpy as jnp
from jax import lax
from jax.sharding import Mesh
from jax.sharding import PartitionSpec as P

EP = ("ep_0", "ep_1")
GRP_EP = ("grp", "ep_0", "ep_1")
epsilon = 1e-06
clamp_limit = 7.0
swish_alpha = 1.702


def cut_along(value, dim, devices):
    before, after = (value.shape[:dim], value.shape[dim + 1 :])
    return jnp.moveaxis(value.reshape(*before, devices, -1, *after), dim, 0)


def laid_out(blocks, dim):
    blocks = jnp.moveaxis(blocks, 0, dim)
    shape = blocks.shape
    return blocks.reshape(*shape[:dim], shape[dim] * shape[dim + 1], *shape[dim + 2 :])


def turned_blocks(blocks, axes, turns):
    inside = blocks.shape[1:]
    whole = blocks.reshape(*(lax.axis_size(a) for a in axes), *inside)
    for k in turns:
        whole = lax.all_to_all(whole, axes[k], k, k, tiled=True)
    return whole.reshape(-1, *inside)


def exchange_by_chip(value, groups, turns, split_dim, concat_dim):
    devices = lax.axis_size(groups[0]) * lax.axis_size(groups[1])
    blocks = cut_along(value, split_dim, devices)
    return laid_out(turned_blocks(blocks, groups, turns), concat_dim)


def sent_and_summed(value, axis, dim):
    blocks = cut_along(value, dim, lax.axis_size(axis))
    arrived = lax.all_to_all(blocks, axis, split_axis=0, concat_axis=0, tiled=True)
    return arrived.astype(jnp.float32).sum(axis=0)


def rms_norm(tokens, norm_gain):
    widened = tokens.astype(jnp.float32)
    scaled = widened * lax.rsqrt(jnp.mean(widened * widened, axis=-1, keepdims=True) + epsilon)
    return (scaled * norm_gain).astype(jnp.bfloat16)


def body(tokens, norm_gain, w_gate, w_up, w_down, expert_ids, gate_weights):
    tok_rows, model_width = tokens.shape
    top_count = expert_ids.shape[1]
    ep_count = lax.axis_size(EP)
    tp_count = lax.axis_size("tp")
    local_experts = w_gate.shape[0]
    experts_all = local_experts * ep_count
    capacity = min(tok_rows, tok_rows * top_count * 4 // (3 * experts_all))
    normed = rms_norm(tokens, norm_gain)
    flat_ids = expert_ids.reshape(-1)
    onehot = (flat_ids[:, None] == jnp.arange(experts_all, dtype=jnp.int32)[None, :]).astype(
        jnp.int32
    )
    before = jnp.cumsum(onehot, axis=0) - onehot
    slot_index = jnp.sum(before * onehot, axis=1)
    dest_row = flat_ids * capacity + slot_index
    owner_tok = jnp.arange(tok_rows * top_count, dtype=jnp.int32) // top_count
    slot_table = (
        jnp.full((experts_all * capacity,), tok_rows, jnp.int32).at[dest_row].set(owner_tok)
    )
    padded = jnp.concatenate([normed, jnp.zeros((1, model_width), jnp.bfloat16)], axis=0)
    send_buffer = padded[slot_table].reshape(experts_all, capacity, model_width)
    col_share = model_width // tp_count
    col_part = lax.dynamic_slice_in_dim(send_buffer, lax.axis_index("tp") * col_share, col_share, 2)
    received = exchange_by_chip(col_part, ("ep_0", "ep_1"), (1, 0), 0, 0)
    received = lax.all_gather(received, "tp", axis=2, tiled=True)
    expert_rows = received.reshape(ep_count, local_experts, capacity, model_width)
    gate_pre = jnp.einsum("sjcd,jdf->sjcf", expert_rows, w_gate, preferred_element_type=jnp.float32)
    up_pre = jnp.einsum("sjcd,jdf->sjcf", expert_rows, w_up, preferred_element_type=jnp.float32)
    gated = jnp.minimum(gate_pre, clamp_limit)
    linear = jnp.clip(up_pre, -clamp_limit, clamp_limit)
    activated = (gated * jax.nn.sigmoid(swish_alpha * gated) * (linear + 1.0)).astype(jnp.bfloat16)
    partial_value = jnp.einsum(
        "sjcf,jfd->sjcd", activated, w_down, preferred_element_type=jnp.float32
    ).astype(jnp.bfloat16)
    summed = sent_and_summed(partial_value, "tp", 3).astype(jnp.bfloat16)
    returned = exchange_by_chip(summed, ("ep_0", "ep_1"), (1, 0), 0, 0)
    returned = returned.reshape(experts_all * capacity, returned.shape[3])
    picked = returned[dest_row].reshape(tok_rows, top_count, returned.shape[1]).astype(jnp.float32)
    return jnp.sum(picked * gate_weights[:, :, None], axis=1).astype(jnp.bfloat16)


def solution(mesh):
    torus = Mesh(
        mesh.devices.reshape(mesh.shape["grp"], 32, 2, mesh.shape["tp"]),
        ("grp", "ep_0", "ep_1", "tp"),
    )
    return jax.shard_map(
        body,
        mesh=torus,
        in_specs=(
            P(GRP_EP, None),
            P(),
            P(EP, None, "tp"),
            P(EP, None, "tp"),
            P(EP, "tp", None),
            P(GRP_EP, None),
            P(GRP_EP, None),
        ),
        out_specs=P(GRP_EP, "tp"),
        check_vma=False,
    )
```

profile of v0, /device:TPU:33, one launch (start us, length us, event | category | flops | bytes accessed | tf_op | source)
XLA Modules:
  0.0 449.6 jit_solution(9208010235505050856)
XLA Ops:
  6.6 0.9 copy.23
  7.7 0.7 broadcast_multiply_fusion
  8.4 1.8 reduce-window.6
  10.2 0.3 slice_reduce_fusion
  10.9 3.4 scatter_custom_fusion
  14.3 1.4 fusion
  15.7 1.4 fusion.2
  17.2 6.0 %gather_fusion = bf16[1024,2048]{1,0:T(8,128)(2,1)} fusion(bf16[193,2048]{1,0:T(8,128)(2,1)S(1)} %concatenate.3, s32[1024]{0:T(1024)S(1)} %fusion.30), kind=kCustom, calls=%fused_computation | custom fusion | bytes 8392704 | tf_op jit(solution)/shard_map/gather | solution.py:72
  23.2 1.3 constant_dynamic-slice_fusion
  24.6 45.8 %all_to_all.25 = bf16[32,2,1,16,512]{4,3,0,2,1:T(8,128)(2,1)S(1)} all-to-all(bf16[32,2,1,16,512]{4,3,0,2,1:T(8,128)(2,1)S(1)} %copy.26), channel_id=1, replica_groups=mesh['grp'=2,'ep_0'=32,'ep_1'=2,'tp'=4] {'ep_1'}, dimensions={1} | all-to-all | bytes 2097152 | tf_op jit(solution)/shard_map/all_to_all | solution.py:29
  70.5 110.0 %all_to_all.26 = bf16[32,2,1,16,512]{4,3,1,2,0:T(8,128)(2,1)} all-to-all(bf16[32,2,1,16,512]{4,3,1,2,0:T(8,128)(2,1)S(1)} %copy.27), channel_id=1, replica_groups=mesh['grp'=2,'ep_0'=32,'ep_1'=2,'tp'=4] {'ep_0'}, dimensions={0} | all-to-all | bytes 2097152 | tf_op jit(solution)/shard_map/all_to_all | solution.py:29
  180.5 51.5 %all-gather.2.cloned.1.call-done = bf16[64,16,2048]{2,1,0:T(8,128)(2,1)} async-done(((bf16[64,16,512]{2,1,0:T(8,128)(2,1)}), bf16[64,16,2048]{2,1,0:T(8,128)(2,1)}) %all-gather.2.cloned.1.call-update) | async-done | bytes 4194320 | tf_op jit(solution)/shard_map/all_gather | solution.py:76
  232.1 4.5 %fusion.3 = f32[64,1,16,256]{3,2,0,1:T(8,128)} fusion(bf16[64,16,2048]{2,1,0:T(8,128)(2,1)} %all-gather.2.cloned.1.call-done, bf16[1,2048,256]{2,1,0:T(8,128)(2,1)S(1)} %copy-done.2), kind=kOutput, calls=%fused_computation.12 | convolution fusion | flops 1074003968 | bytes 6291456 | tf_op jit(solution)/shard_map/sjcd,jdf->sjcf/dot_general | solution.py:78
  236.6 8.9 %convolution_convert_fusion = bf16[64,16,2048]{2,1,0:T(8,128)(2,1)} fusion(bf16[64,16,2048]{2,1,0:T(8,128)(2,1)} %all-gather.2.cloned.1.call-done, bf16[1,256,2048]{2,1,0:T(8,128)(2,1)S(1)} %copy-done, bf16[1,2048,256]{2,1,0:T(8,128)(2,1)S(1)} %copy-done.3, f32[64,1,16,256]{3,2,0,1:T(8,128)} %fusion.3), kind=kOutput, calls=%fused_computation.4 | convolution fusion | flops 2151940096 | bytes 11534336 | tf_op jit(solution)/shard_map/sjcf,jfd->sjcd/dot_general | solution.py:83
  245.4 2.8 copy.36
  248.3 51.3 %all_to_all.27 = bf16[4,64,1,16,512]{4,3,1,2,0:T(8,128)(2,1)} all-to-all(bf16[4,64,1,16,512]{4,3,1,2,0:T(8,128)(2,1)S(1)} %bitcast.77), channel_id=1, replica_groups=mesh['grp'=2,'ep_0'=32,'ep_1'=2,'tp'=4] {'tp'}, dimensions={0} | all-to-all | bytes 8388608 | tf_op jit(solution)/shard_map/all_to_all | solution.py:41
  299.6 3.3 reduce_sum.44
  303.0 6.1 %all_to_all.28 = bf16[32,2,1,1,16,512]{5,4,0,3,2,1:T(8,128)(2,1)S(1)} all-to-all(bf16[32,2,1,1,16,512]{5,4,0,3,2,1:T(8,128)(2,1)S(1)} %copy.29), channel_id=1, replica_groups=mesh['grp'=2,'ep_0'=32,'ep_1'=2,'tp'=4] {'ep_1'}, dimensions={1} | all-to-all | bytes 2097152 | tf_op jit(solution)/shard_map/all_to_all | solution.py:29
  309.1 1.1 copy.30
  310.2 23.4 %all-to-all-start.4 = ((bf16[32,2,1,1,16,512]{5,4,1,3,2,0:T(8,128)(2,1)}), bf16[32,2,1,1,16,512]{5,4,1,3,2,0:T(8,128)(2,1)S(1)}, u32[]{:S(2)}, u32[]{:S(2)}) async-start(bf16[32,2,1,1,16,512]{5,4,1,3,2,0:T(8,128)(2,1)} %copy.30), calls=%async_computation.4 | async-start | bytes 2097152 | tf_op jit(solution)/shard_map/all_to_all | solution.py:29
  333.7 104.2 %all-to-all-done.4 = bf16[32,2,1,1,16,512]{5,4,1,3,2,0:T(8,128)(2,1)S(1)} async-done(((bf16[32,2,1,1,16,512]{5,4,1,3,2,0:T(8,128)(2,1)}), bf16[32,2,1,1,16,512]{5,4,1,3,2,0:T(8,128)(2,1)S(1)}, u32[]{:S(2)}, u32[]{:S(2)}) %all-to-all-start.4) | async-done | bytes 1048608 | tf_op jit(solution)/shard_map/all_to_all | solution.py:29
  437.9 2.7 gather_fusion.1
  440.6 0.5 reshape.102
  441.1 1.7 multiply_reduce_fusion
  (27 shorter events, 1.2 us)
Async XLA Ops:
  6.5 230.0 %copy-start = (bf16[1,256,2048]{2,1,0:T(8,128)(2,1)S(1)}, bf16[1,256,2048]{2,1,0:T(8,128)(2,1)}, u32[]{:S(2)}) copy-start(bf16[1,256,2048]{2,1,0:T(8,128)(2,1)} %param.11) | copy-start | bytes 3145732
  6.6 225.5 %all-gather.2.cloned.1.call-start = ((), (), s32[]{:S(2)}) async-start(), calls=%async_computation.5 | async-start | bytes 5242880 | tf_op jit(solution)/shard_map/all_gather | solution.py:76
  24.6 207.5 %copy-start.2 = (bf16[1,2048,256]{2,1,0:T(8,128)(2,1)S(1)}, bf16[1,2048,256]{2,1,0:T(8,128)(2,1)}, u32[]{:S(2)}) copy-start(bf16[1,2048,256]{2,1,0:T(8,128)(2,1)} %param.9) | copy-start | bytes 3145732
  180.5 56.1 %copy-start.3 = (bf16[1,2048,256]{2,1,0:T(8,128)(2,1)S(1)}, bf16[1,2048,256]{2,1,0:T(8,128)(2,1)}, u32[]{:S(2)}) copy-start(bf16[1,2048,256]{2,1,0:T(8,128)(2,1)} %param.10) | copy-start | bytes 3145732
  302.9 30.7 %copy-start.1 = (f32[192,4]{0,1:T(4,128)S(1)}, f32[192,4]{0,1:T(4,128)}, u32[]{:S(2)}) copy-start(f32[192,4]{0,1:T(4,128)} %param.13) | copy-start | bytes 9220
  310.2 127.7 %all-to-all-start.4 = ((bf16[32,2,1,1,16,512]{5,4,1,3,2,0:T(8,128)(2,1)}), bf16[32,2,1,1,16,512]{5,4,1,3,2,0:T(8,128)(2,1)S(1)}, u32[]{:S(2)}, u32[]{:S(2)}) async-start(bf16[32,2,1,1,16,512]{5,4,1,3,2,0:T(8,128)(2,1)} %copy.30), calls=%async_computation.4 | async-start | bytes 2097152 | tf_op jit(solution)/shard_map/all_to_all | solution.py:29
Sparse Core Ops, SparseCore 0:
  180.7 51.3 all-gather.1
where the time goes:
time: 450 us
  blocking collectives  213 us (47%)
  waiting for transfers between devices  156 us (35%)
  starting transfers between devices  23.4 us (5%)
  local copies, waits for them, and re-layouts  19.8 us (4%)
  between operations  13.6 us (3%)
  matrix products  13.4 us (3%)
  other arithmetic  10.5 us (2%)
    all_to_all x3, blocking collectives, turned_blocks(): whole = lax.all_to_all(whole, axes[k], k, k, tiled=True)  162 us
    all_to_all x1, waiting for transfers between devices, turned_blocks(): whole = lax.all_to_all(whole, axes[k], k, k, tiled=True)  104 us
    all_gather x1, waiting for transfers between devices, body(): received = lax.all_gather(received, 'tp', axis=2, tiled=True)  51.5 us
    all_to_all x1, blocking collectives, sent_and_summed(): lax.all_to_all(blocks, axis, split_axis=0, concat_axis=0, tiled=True)  51.3 us
    all_to_all x1, starting transfers between devices, turned_blocks(): whole = lax.all_to_all(whole, axes[k], k, k, tiled=True)  23.4 us
  transfers between devices with their start and end apart: 2, of which 2 were waited for; matrix products, arithmetic and copies ran while one was open for 0% of the time, Pallas kernels for 0%

commit v1 on v0

--- a/solution.py
+++ b/solution.py
@@ -73,7 +73,9 @@
     col_share = model_width // tp_count
     col_part = lax.dynamic_slice_in_dim(send_buffer, lax.axis_index("tp") * col_share, col_share, 2)
     received = exchange_by_chip(col_part, ("ep_0", "ep_1"), (1, 0), 0, 0)
-    received = lax.all_gather(received, "tp", axis=2, tiled=True)
+    received = jnp.concatenate(
+        lax.all_to_all(jnp.stack([received] * lax.axis_size("tp")), "tp", 0, 0), axis=2
+    )
     expert_rows = received.reshape(ep_count, local_experts, capacity, model_width)
     gate_pre = jnp.einsum("sjcd,jdf->sjcf", expert_rows, w_gate, preferred_element_type=jnp.float32)
     up_pre = jnp.einsum("sjcd,jdf->sjcf", expert_rows, w_up, preferred_element_type=jnp.float32)

time: 450 us -> 422 us (0.938)
  blocking collectives: 213 us -> 265 us
  waiting for transfers between devices: 156 us -> 105 us
  starting transfers between devices: 23.4 us -> 7.93 us
  between operations: 13.6 us -> 0.23 us
    all_to_all x0 -> x1, blocking collectives: none -> 52 us  [body(): lax.all_to_all(jnp.stack([received] * lax.axis_size('tp')), 'tp', 0, 0)]
    all_gather x1 -> x0, waiting for transfers between devices: 51.5 us -> none  [body(): received = lax.all_gather(received, 'tp', axis=2, tiled=True)]
    all_to_all x1, starting transfers between devices: 23.4 us -> 7.93 us  [turned_blocks(): whole = lax.all_to_all(whole, axes[k], k, k, tiled=True)]
  transfers between devices with their start and end apart: 2 -> 1, of which waited for: 2 -> 1; matrix products, arithmetic and copies ran while one was open for 0% -> 0% of each run, Pallas kernels for 0% -> 0%
where the time goes in v1:
time: 422 us; the launch traced here: 421 us
  blocking collectives  265 us (63%)
  waiting for transfers between devices  105 us (25%)
  local copies, waits for them, and re-layouts  22.9 us (5%)
  other arithmetic  10.5 us (2%)
  matrix products  9.82 us (2%)
  starting transfers between devices  7.93 us (2%)
    all_to_all x3, blocking collectives, turned_blocks(): whole = lax.all_to_all(whole, axes[k], k, k, tiled=True)  163 us
    all_to_all x1, waiting for transfers between devices, turned_blocks(): whole = lax.all_to_all(whole, axes[k], k, k, tiled=True)  105 us
    all_to_all x1, blocking collectives, body(): lax.all_to_all(jnp.stack([received] * lax.axis_size('tp')), 'tp', 0, 0)  52 us
    all_to_all x1, blocking collectives, sent_and_summed(): lax.all_to_all(blocks, axis, split_axis=0, concat_axis=0, tiled=True)  50.5 us
    dot_general x1, matrix products, body(): jnp.einsum('sjcf,jfd->sjcd', activated, w_down, preferred_element_type=jn...  8.57 us
  transfers between devices with their start and end apart: 1, of which 1 were waited for; matrix products, arithmetic and copies ran while one was open for 0% of the time, Pallas kernels for 0%

profile of v1, /device:TPU:33, one launch (start us, length us, event | category | flops | bytes accessed | tf_op | source)
XLA Modules:
  0.0 420.9 jit_solution(46805678572778544)
XLA Ops:
  0.0 0.9 copy.24
  1.1 0.7 broadcast_multiply_fusion
  1.8 1.8 reduce-window.6
  4.3 3.4 scatter_custom_fusion
  7.7 1.4 fusion
  9.1 1.4 fusion.2
  10.6 6.0 %gather_fusion = bf16[1024,2048]{1,0:T(8,128)(2,1)} fusion(bf16[193,2048]{1,0:T(8,128)(2,1)S(1)} %concatenate.3, s32[1024]{0:T(1024)S(1)} %fusion.30), kind=kCustom, calls=%fused_computation | custom fusion | bytes 8392704 | tf_op jit(solution)/shard_map/gather | solution.py:72
  16.6 1.3 constant_dynamic-slice_fusion
  18.0 45.6 %all_to_all.30 = bf16[32,2,1,16,512]{4,3,0,2,1:T(8,128)(2,1)S(1)} all-to-all(bf16[32,2,1,16,512]{4,3,0,2,1:T(8,128)(2,1)S(1)} %copy.27), channel_id=1, replica_groups=mesh['grp'=2,'ep_0'=32,'ep_1'=2,'tp'=4] {'ep_1'}, dimensions={1} | all-to-all | bytes 2097152 | tf_op jit(solution)/shard_map/all_to_all | solution.py:29
  63.8 109.9 %all_to_all.31 = bf16[32,2,1,16,512]{4,3,1,2,0:T(8,128)(2,1)S(1)} all-to-all(bf16[32,2,1,16,512]{4,3,1,2,0:T(8,128)(2,1)S(1)} %copy.28), channel_id=1, replica_groups=mesh['grp'=2,'ep_0'=32,'ep_1'=2,'tp'=4] {'ep_0'}, dimensions={0} | all-to-all | bytes 2097152 | tf_op jit(solution)/shard_map/all_to_all | solution.py:29
  174.2 52.0 %all_to_all.32 = bf16[4,64,16,512]{3,2,1,0:T(8,128)(2,1)S(1)} all-to-all(bf16[4,64,16,512]{3,2,1,0:T(8,128)(2,1)S(1)} %stack.3), channel_id=1, replica_groups=mesh['grp'=2,'ep_0'=32,'ep_1'=2,'tp'=4] {'tp'}, dimensions={0} | all-to-all | bytes 8388608 | tf_op jit(solution)/shard_map/all_to_all | solution.py:77
  226.2 0.6 copy.36
  226.9 1.9 copy-done.1
  228.8 1.3 fusion.3
  230.1 8.6 %convolution_convert_fusion = bf16[64,16,2048]{2,1,0:T(8,128)(2,1)} fusion(bf16[64,16,2048]{2,1,0:T(8,128)(2,1)} %bitcast.86, bf16[1,256,2048]{2,1,0:T(8,128)(2,1)S(1)} %copy-done, bf16[1,2048,256]{2,1,0:T(8,128)(2,1)S(1)} %copy-done.4, f32[64,1,16,256]{3,2,0,1:T(8,128)S(1)} %fusion.3), kind=kOutput, calls=%fused_computation.4 | convolution fusion | flops 2151940096 | bytes 11534336 | tf_op jit(solution)/shard_map/sjcf,jfd->sjcd/dot_general | solution.py:85
  238.7 2.8 copy.39
  241.5 50.5 %all_to_all.33 = bf16[4,64,1,16,512]{4,3,1,2,0:T(8,128)(2,1)} all-to-all(bf16[4,64,1,16,512]{4,3,1,2,0:T(8,128)(2,1)S(1)} %bitcast.81), channel_id=1, replica_groups=mesh['grp'=2,'ep_0'=32,'ep_1'=2,'tp'=4] {'tp'}, dimensions={0} | all-to-all | bytes 8388608 | tf_op jit(solution)/shard_map/all_to_all | solution.py:41
  292.0 3.3 reduce_sum.44
  295.4 6.9 %all_to_all.34 = bf16[32,2,1,1,16,512]{5,4,0,3,2,1:T(8,128)(2,1)S(1)} all-to-all(bf16[32,2,1,1,16,512]{5,4,0,3,2,1:T(8,128)(2,1)S(1)} %copy.31), channel_id=1, replica_groups=mesh['grp'=2,'ep_0'=32,'ep_1'=2,'tp'=4] {'ep_1'}, dimensions={1} | all-to-all | bytes 2097152 | tf_op jit(solution)/shard_map/all_to_all | solution.py:29
  302.4 1.1 copy.32
  303.4 7.9 %all-to-all-start.5 = ((bf16[32,2,1,1,16,512]{5,4,1,3,2,0:T(8,128)(2,1)}), bf16[32,2,1,1,16,512]{5,4,1,3,2,0:T(8,128)(2,1)S(1)}, u32[]{:S(2)}, u32[]{:S(2)}) async-start(bf16[32,2,1,1,16,512]{5,4,1,3,2,0:T(8,128)(2,1)} %copy.32), calls=%async_computation.5 | async-start | bytes 2097152 | tf_op jit(solution)/shard_map/all_to_all | solution.py:29
  311.5 104.5 %all-to-all-done.5 = bf16[32,2,1,1,16,512]{5,4,1,3,2,0:T(8,128)(2,1)S(1)} async-done(((bf16[32,2,1,1,16,512]{5,4,1,3,2,0:T(8,128)(2,1)}), bf16[32,2,1,1,16,512]{5,4,1,3,2,0:T(8,128)(2,1)S(1)}, u32[]{:S(2)}, u32[]{:S(2)}) %all-to-all-start.5) | async-done | bytes 1048608 | tf_op jit(solution)/shard_map/all_to_all | solution.py:29
  416.0 2.7 gather_fusion.1
  419.2 1.7 multiply_reduce_fusion
  (29 shorter events, 2.4 us)
Async XLA Ops:
  0.0 230.1 %copy-start = (bf16[1,256,2048]{2,1,0:T(8,128)(2,1)S(1)}, bf16[1,256,2048]{2,1,0:T(8,128)(2,1)}, u32[]{:S(2)}) copy-start(bf16[1,256,2048]{2,1,0:T(8,128)(2,1)} %param.11) | copy-start | bytes 3145732
  226.2 2.6 copy-start.3
  226.9 1.9 copy-start.1
  226.9 3.2 copy-start.4
  295.3 16.1 %copy-start.2 = (f32[192,4]{0,1:T(4,128)S(1)}, f32[192,4]{0,1:T(4,128)}, u32[]{:S(2)}) copy-start(f32[192,4]{0,1:T(4,128)} %param.13) | copy-start | bytes 9220
  303.4 112.6 %all-to-all-start.5 = ((bf16[32,2,1,1,16,512]{5,4,1,3,2,0:T(8,128)(2,1)}), bf16[32,2,1,1,16,512]{5,4,1,3,2,0:T(8,128)(2,1)S(1)}, u32[]{:S(2)}, u32[]{:S(2)}) async-start(bf16[32,2,1,1,16,512]{5,4,1,3,2,0:T(8,128)(2,1)} %copy.32), calls=%async_computation.5 | async-start | bytes 2097152 | tf_op jit(solution)/shard_map/all_to_all | solution.py:29
